TPU v7x, 32 devices: a whole 2x2x4 slice. The times are simulated.
32 devices in a mesh: sp: 8 (over z, x), tp: 4 (over y, core).
Axes of the slice: x: 2, y: 2, z: 4, core: 2. Of those that a mesh axis runs over, the one named last changes fastest.
Arguments:
- inputs: bfloat16 [4096, 2048], P('sp', 'tp'), may hold values from -45 to 45
- norm_gain: float32 [3, 2048], replicated, may hold values from 0.1 to 1.9
- w_value: bfloat16 [3, 2048, 1024], P(None, 'sp', 'tp'), may hold values from -0.125 to 0.125
- w_gate: bfloat16 [3, 2048, 1024], P(None, 'sp', 'tp'), may hold values from -0.125 to 0.125
- conv_taps: float32 [3, 31, 1024], P(None, None, 'tp'), may hold values from -5 to 5
- ln_gain: float32 [3, 1024], P(None, 'tp'), may hold values from 0.1 to 1.9
- ln_bias: float32 [3, 1024], P(None, 'tp'), may hold values from -3 to 3
- w_out: bfloat16 [3, 1024, 2048], P(None, 'tp', 'sp'), may hold values from -0.1875 to 0.1875
Outputs:
- stream: bfloat16 [4096, 2048], P('sp', 'tp')
All inputs are finite; a program needn't handle non-finite values.
Results may differ from a plain program's by a relative error of at most 0.01.
Values may be sent and summed in bfloat16 or wider, within the bound.
A program may use at most 64 MiB of HBM per device.

v0:
```python
import jax
import jax.numpy as jnp
from jax import lax
from jax.sharding import PartitionSpec as P


def from_behind(block, axis, distance):
    devices = range(lax.axis_size(axis))
    route = [(i - distance, i) for i in devices if i - distance in devices]
    return lax.ppermute(block, axis, route)


def shards(inputs, norm_gain, w_value, w_gate, conv_taps, ln_gain, ln_bias, w_out):
    rows = inputs.shape[0]
    reach = conv_taps.shape[1] - 1
    layers = conv_taps.shape[0]
    channels = conv_taps.shape[2] * lax.axis_size("tp")
    whole_value, whole_gate, whole_out = (
        lax.all_gather(w_value, "sp", axis=1, tiled=True),
        lax.all_gather(w_gate, "sp", axis=1, tiled=True),
        lax.all_gather(w_out, "sp", axis=2, tiled=True),
    )
    stream = inputs
    for layer in range(layers):
        full_rows = lax.all_gather(stream, "tp", axis=1, tiled=True)
        xf = full_rows.astype(jnp.float32)
        meansq = jnp.mean(xf * xf, axis=1, keepdims=True)
        hidden = (xf * lax.rsqrt(meansq + 1e-06) * norm_gain[layer][None, :]).astype(jnp.bfloat16)
        value = jnp.dot(hidden, whole_value[layer], preferred_element_type=jnp.float32)
        gate = jnp.dot(hidden, whole_gate[layer], preferred_element_type=jnp.float32)
        glu = (value * jax.nn.sigmoid(gate)).astype(jnp.bfloat16)
        rim = from_behind(glu[rows - reach :], "sp", 1)
        padded = jnp.concatenate([rim, glu], axis=0)
        count = padded.shape[0] - reach
        filtered = jnp.zeros((count, glu.shape[1]), jnp.float32)
        for tap in range(reach + 1):
            filtered = filtered + conv_taps[layer, tap][None, :] * padded[tap : tap + count].astype(
                jnp.float32
            )
        total_sum, total_sq = lax.psum(
            (jnp.sum(filtered, axis=1), jnp.sum(filtered * filtered, axis=1)), "tp"
        )
        mean_val = (total_sum / channels)[:, None]
        var_val = (total_sq / channels)[:, None] - mean_val * mean_val
        normed = jax.nn.silu(
            (filtered - mean_val) * lax.rsqrt(var_val + 1e-06) * ln_gain[layer][None, :]
            + ln_bias[layer][None, :]
        ).astype(jnp.bfloat16)
        partial_out = jnp.dot(normed, whole_out[layer], preferred_element_type=jnp.float32)
        summed = lax.psum_scatter(
            partial_out.astype(jnp.bfloat16), "tp", scatter_dimension=1, tiled=True
        ).astype(jnp.float32)
        kept = stream.astype(jnp.float32)
        stream = (kept + summed).astype(jnp.bfloat16)
    return stream


def solution(mesh):
    in_specs = (
        P("sp", "tp"),
        P(),
        P(None, "sp", "tp"),
        P(None, "sp", "tp"),
        P(None, None, "tp"),
        P(None, "tp"),
        P(None, "tp"),
        P(None, "tp", "sp"),
    )
    out_specs = P("sp", "tp")
    return jax.shard_map(shards, mesh=mesh, in_specs=in_specs, out_specs=out_specs, check_vma=False)
```

profile of v0, /device:TPU:0, one launch (start us, length us, event | category | flops | bytes accessed | tf_op | source)
XLA Modules:
  0.0 422.9 jit_solution(3484355526385756584)
XLA Ops:
  13.1 21.1 %all-gather.7.cloned.1.call-done = bf16[512,2048]{1,0:T(8,128)(2,1)} async-done(((bf16[512,512]{1,0:T(8,128)(2,1)}), bf16[512,2048]{1,0:T(8,128)(2,1)}) %all-gather.7.cloned.1.call-update) | async-done | bytes 2097168 | tf_op jit(solution)/shard_map/all_gather | solution.py:25
  36.3 60.1 %all-gather.11.cloned.1.call-done = bf16[3,2048,256]{2,1,0:T(8,128)(2,1)} async-done(((bf16[3,256,256]{2,1,0:T(8,128)(2,1)}), bf16[3,2048,256]{2,1,0:T(8,128)(2,1)}) %all-gather.11.cloned.1.call-update) | async-done | bytes 3145744 | tf_op jit(solution)/shard_map/all_gather | solution.py:20
  96.4 2.8 fusion.17
  99.2 58.1 %all-gather.9.cloned.1.call-done = bf16[3,2048,256]{2,1,0:T(8,128)(2,1)} async-done(((bf16[3,256,256]{2,1,0:T(8,128)(2,1)}), bf16[3,2048,256]{2,1,0:T(8,128)(2,1)}) %all-gather.9.cloned.1.call-update) | async-done | bytes 3145744 | tf_op jit(solution)/shard_map/all_gather | solution.py:19
  159.4 2.5 collective-permute-start
  163.3 2.4 fusion.134
  165.7 5.7 %all-reduce.2 = (f32[512]{0:T(512)S(1)}, f32[512]{0:T(512)S(1)}) all-reduce(f32[512]{0:T(512)S(1)} %get-tuple-element.10, f32[512]{0:T(512)S(1)} %get-tuple-element.9), channel_id=1, replica_groups=mesh['sp'=8,'tp'=4] {'tp'}, use_global_device_ids=true, to_apply=%region_4.0 | all-reduce | flops 1024 | bytes 8192 | tf_op jit(solution)/shard_map/psum | solution.py:40
  171.4 49.2 %all-gather.13.cloned.1.call-done = bf16[3,256,2048]{2,1,0:T(8,128)(2,1)} async-done(((bf16[3,256,256]{2,1,0:T(8,128)(2,1)}), bf16[3,256,2048]{2,1,0:T(8,128)(2,1)}) %all-gather.13.cloned.1.call-update) | async-done | bytes 3145744 | tf_op jit(solution)/shard_map/all_gather | solution.py:21
  220.6 3.4 convolution_convert_fusion.2
  224.1 29.5 %reduce-scatter.4.cloned.1.call-done = bf16[512,512]{1,0:T(8,128)(2,1)} async-done(((bf16[512,2048]{1,0:T(8,128)(2,1)}), bf16[512,512]{1,0:T(8,128)(2,1)}) %reduce-scatter.4.cloned.1.call-update) | async-done | bytes 524304 | tf_op jit(solution)/shard_map/reduce_scatter | solution.py:50
  255.6 22.6 %all-gather.15.cloned.1.call-done = bf16[512,2048]{1,0:T(8,128)(2,1)} async-done(((bf16[512,512]{1,0:T(8,128)(2,1)}), bf16[512,2048]{1,0:T(8,128)(2,1)}) %all-gather.15.cloned.1.call-update) | async-done | bytes 2097168 | tf_op jit(solution)/shard_map/all_gather | solution.py:25
  280.4 2.8 fusion.14
  285.2 3.4 collective-permute-start.1
  290.0 2.4 fusion.133
  292.4 6.0 %all-reduce.1 = (f32[512]{0:T(512)S(1)}, f32[512]{0:T(512)S(1)}) all-reduce(f32[512]{0:T(512)S(1)} %get-tuple-element.8, f32[512]{0:T(512)S(1)} %get-tuple-element.7), channel_id=1, replica_groups=mesh['sp'=8,'tp'=4] {'tp'}, use_global_device_ids=true, to_apply=%region_10.11 | all-reduce | flops 1024 | bytes 8192 | tf_op jit(solution)/shard_map/psum | solution.py:40
  298.4 3.4 convolution_convert_fusion.1
  301.9 32.1 %reduce-scatter.6.cloned.1.call-done = bf16[512,512]{1,0:T(8,128)(2,1)} async-done(((bf16[512,2048]{1,0:T(8,128)(2,1)}), bf16[512,512]{1,0:T(8,128)(2,1)}) %reduce-scatter.6.cloned.1.call-update) | async-done | bytes 524304 | tf_op jit(solution)/shard_map/reduce_scatter | solution.py:50
  336.0 22.7 %all-gather.17.cloned.1.call-done = bf16[512,2048]{1,0:T(8,128)(2,1)} async-done(((bf16[512,512]{1,0:T(8,128)(2,1)}), bf16[512,2048]{1,0:T(8,128)(2,1)}) %all-gather.17.cloned.1.call-update) | async-done | bytes 2097168 | tf_op jit(solution)/shard_map/all_gather | solution.py:25
  360.8 2.8 fusion.11
  365.6 3.6 collective-permute-start.2
  370.4 2.4 fusion.132
  372.8 5.9 %all-reduce = (f32[512]{0:T(512)S(1)}, f32[512]{0:T(512)S(1)}) all-reduce(f32[512]{0:T(512)S(1)} %get-tuple-element.6, f32[512]{0:T(512)S(1)} %get-tuple-element.5), channel_id=1, replica_groups=mesh['sp'=8,'tp'=4] {'tp'}, use_global_device_ids=true, to_apply=%region_16.17 | all-reduce | flops 1024 | bytes 8192 | tf_op jit(solution)/shard_map/psum | solution.py:40
  378.8 3.4 convolution_convert_fusion
  382.2 32.1 %reduce-scatter.8.cloned.1.call-done = bf16[512,512]{1,0:T(8,128)(2,1)} async-done(((bf16[512,2048]{1,0:T(8,128)(2,1)}), bf16[512,512]{1,0:T(8,128)(2,1)}) %reduce-scatter.8.cloned.1.call-update) | async-done | bytes 524304 | tf_op jit(solution)/shard_map/reduce_scatter | solution.py:50
  (63 shorter events, 29.1 us)
Async XLA Ops:
  6.5 27.7 %all-gather.7.cloned.1.call-start = ((), (), s32[]{:S(2)}) async-start(), calls=%async_computation.3 | async-start | bytes 2621440 | tf_op jit(solution)/shard_map/all_gather | solution.py:25
  7.3 89.2 %all-gather.11.cloned.1.call-start = ((), (), s32[]{:S(2)}) async-start(), calls=%async_computation.5 | async-start | bytes 3538944 | tf_op jit(solution)/shard_map/all_gather | solution.py:20
  8.0 149.3 %all-gather.9.cloned.1.call-start = ((), (), s32[]{:S(2)}) async-start(), calls=%async_computation.4 | async-start | bytes 3538944 | tf_op jit(solution)/shard_map/all_gather | solution.py:19
  8.7 211.9 %all-gather.13.cloned.1.call-start = ((), (), s32[]{:S(2)}) async-start(), calls=%async_computation.6 | async-start | bytes 3538944 | tf_op jit(solution)/shard_map/all_gather | solution.py:21
  9.3 244.2 %reduce-scatter.4.cloned.1.call-start = ((), (), s32[]{:S(2)}) async-start(), calls=%async_computation.7 | async-start | bytes 2621440 | tf_op jit(solution)/shard_map/reduce_scatter | solution.py:50
  96.4 60.9 %copy-start.3 = (bf16[512,2048]{1,0:T(8,128)(2,1)S(1)}, bf16[512,2048]{1,0:T(8,128)(2,1)}, u32[]{:S(2)}) copy-start(bf16[512,2048]{1,0:T(8,128)(2,1)} %all-gather.7.cloned.1.call-done) | copy-start | bytes 6291460
  99.2 62.6 %copy-start.7 = (f32[3,256]{1,0:T(4,128)S(1)}, f32[3,256]{1,0:T(4,128)}, u32[]{:S(2)}) copy-start(f32[3,256]{1,0:T(4,128)} %param.14) | copy-start | bytes 9220
  159.4 3.9 collective-permute-start
  220.6 33.0 %copy-start.2 = (bf16[512,512]{1,0:T(8,128)(2,1)S(1)}, bf16[512,512]{1,0:T(8,128)(2,1)}, u32[]{:S(2)}) copy-start(bf16[512,512]{1,0:T(8,128)(2,1)} %param.8) | copy-start | bytes 1572868
  224.0 31.6 %copy-start.6 = (f32[3,31,256]{2,1,0:T(8,128)S(1)}, f32[3,31,256]{2,1,0:T(8,128)}, u32[]{:S(2)}) copy-start(f32[3,31,256]{2,1,0:T(8,128)} %param.12) | copy-start | bytes 285700
  224.0 54.3 %all-gather.15.cloned.1.call-start = ((), (), s32[]{:S(2)}) async-start(), calls=%async_computation.8 | async-start | bytes 2621440 | tf_op jit(solution)/shard_map/all_gather | solution.py:25
  255.6 78.4 %reduce-scatter.6.cloned.1.call-start = ((), (), s32[]{:S(2)}) async-start(), calls=%async_computation.9 | async-start | bytes 2621440 | tf_op jit(solution)/shard_map/reduce_scatter | solution.py:50
  280.4 2.8 copy-start.4
  285.2 4.8 %collective-permute-start.1 = (bf16[30,256]{1,0:T(8,128)(2,1)S(1)}, bf16[30,256]{1,0:T(8,128)(2,1)S(1)}, u32[]{:S(2)}, u32[]{:S(2)}) collective-permute-start(bf16[30,256]{1,0:T(8,128)(2,1)S(1)} %slice.880), channel_id=1, source_target_pairs={{0,4},{4,8},{8,12},{12,16},{16,20},{20,24},{24,28},{1,5},{5,9},{9,... | collective-permute-start | bytes 46088 | tf_op jit(solution)/shard_map/ppermute | solution.py:10
  298.4 35.5 %copy-start = (bf16[512,512]{1,0:T(8,128)(2,1)S(1)}, bf16[512,512]{1,0:T(8,128)(2,1)}, u32[]{:S(2)}) copy-start(bf16[512,512]{1,0:T(8,128)(2,1)} %add_convert_fusion.2) | copy-start | bytes 1572868
  301.8 56.8 %all-gather.17.cloned.1.call-start = ((), (), s32[]{:S(2)}) async-start(), calls=%async_computation.10 | async-start | bytes 2621440 | tf_op jit(solution)/shard_map/all_gather | solution.py:25
  336.0 78.4 %reduce-scatter.8.cloned.1.call-start = ((), (), s32[]{:S(2)}) async-start(), calls=%async_computation.11 | async-start | bytes 2621440 | tf_op jit(solution)/shard_map/reduce_scatter | solution.py:50
  360.8 2.8 copy-start.5
  365.6 4.8 %collective-permute-start.2 = (bf16[30,256]{1,0:T(8,128)(2,1)S(1)}, bf16[30,256]{1,0:T(8,128)(2,1)S(1)}, u32[]{:S(2)}, u32[]{:S(2)}) collective-permute-start(bf16[30,256]{1,0:T(8,128)(2,1)S(1)} %slice.942), channel_id=1, source_target_pairs={{0,4},{4,8},{8,12},{12,16},{16,20},{20,24},{24,28},{1,5},{5,9},{9,... | collective-permute-start | bytes 46088 | tf_op jit(solution)/shard_map/ppermute | solution.py:10
  378.8 35.6 %copy-start.1 = (bf16[512,512]{1,0:T(8,128)(2,1)S(1)}, bf16[512,512]{1,0:T(8,128)(2,1)}, u32[]{:S(2)}) copy-start(bf16[512,512]{1,0:T(8,128)(2,1)} %add_convert_fusion.1) | copy-start | bytes 1572868
Sparse Core Ops, SparseCore 0:
  8.9 25.2 all-gather.6
  36.4 60.0 all-gather.10
  98.6 58.6 all-gather.8
  159.2 61.3 all-gather.12
  224.1 29.3 reduce-scatter.3
  255.7 22.5 all-gather.14
  302.0 31.9 reduce-scatter.5
  336.1 22.5 all-gather.16
  382.4 31.9 reduce-scatter.7
where the time goes:
time: 424 us; the launch traced here: 423 us
  waiting for transfers between devices  334 us (79%)
  matrix products  24.6 us (6%)
  other arithmetic  19.5 us (5%)
  blocking collectives  17.6 us (4%)
  between operations  13.4 us (3%)
  starting transfers between devices  9.7 us (2%)
    reduce_scatter x3, waiting for transfers between devices, shards(): lax.psum_scatter(partial_out.astype(jnp.bfloat16), 'tp', scatter_dimensio...  93.7 us
    all_gather x3, waiting for transfers between devices, shards(): full_rows = lax.all_gather(stream, 'tp', axis=1, tiled=True)  66.4 us
    all_gather x1, waiting for transfers between devices, shards(): lax.all_gather(w_gate, 'sp', axis=1, tiled=True)  60.1 us
    all_gather x1, waiting for transfers between devices, shards(): lax.all_gather(w_value, 'sp', axis=1, tiled=True)  58.1 us
    all_gather x1, waiting for transfers between devices, shards(): lax.all_gather(w_out, 'sp', axis=2, tiled=True)  49.2 us
    psum x3, blocking collectives, shards(): lax.psum((jnp.sum(filtered, axis=1), jnp.sum(filtered * filtered, axis=1)...  17.6 us
    dot_general x3, matrix products, shards(): jnp.dot(normed, whole_out[layer], preferred_element_type=jnp.float32)  10.2 us
    ppermute x3, starting transfers between devices, from_behind(): return lax.ppermute(block, axis, route)  9.38 us
  transfers between devices with their start and end apart: 12, of which 12 were waited for; matrix products, arithmetic and copies ran while one was open for 3% of the time, Pallas kernels for 0%

commit v1 on v0

--- a/solution.py
+++ b/solution.py
@@ -1,7 +1,20 @@
+import functools
 import jax
 import jax.numpy as jnp
 from jax import lax
 from jax.sharding import PartitionSpec as P
+
+
+def track_ladders_on_mesh(message, on_dim):
+    return jnp.concatenate(
+        lax.all_to_all(
+            jnp.stack([message for _ in range(lax.axis_size("sp"))], axis=0), "sp", 0, 0
+        ),
+        axis=on_dim,
+    )
+
+
+lanes_write = functools.partial(track_ladders_on_mesh, on_dim=1)
 
 
 def from_behind(block, axis, distance):
@@ -16,7 +29,7 @@
     layers = conv_taps.shape[0]
     channels = conv_taps.shape[2] * lax.axis_size("tp")
     whole_value, whole_gate, whole_out = (
-        lax.all_gather(w_value, "sp", axis=1, tiled=True),
+        lanes_write(w_value),
         lax.all_gather(w_gate, "sp", axis=1, tiled=True),
         lax.all_gather(w_out, "sp", axis=2, tiled=True),
     )

time: 424 us -> 392 us (0.925)
  waiting for transfers between devices: 334 us -> 296 us
  starting transfers between devices: 9.7 us -> 18 us
    all_to_all x0 -> x1, waiting for transfers between devices: none -> 79.5 us  [track_ladders_on_mesh(): lax.all_to_all(jnp.stack([message for _ in range(lax.axis_size('sp'))], a...]
    all_gather x1 -> x0, waiting for transfers between devices: 58.1 us -> none  [shards(): lax.all_gather(w_value, 'sp', axis=1, tiled=True)]
    all_gather x1, waiting for transfers between devices: 60.1 us -> 10.2 us  [shards(): lax.all_gather(w_gate, 'sp', axis=1, tiled=True)]
    all_to_all x0 -> x1, starting transfers between devices: none -> 7.41 us  [track_ladders_on_mesh(): lax.all_to_all(jnp.stack([message for _ in range(lax.axis_size('sp'))], a...]
    all_gather x3, waiting for transfers between devices: 66.4 us -> 60 us  [shards(): full_rows = lax.all_gather(stream, 'tp', axis=1, tiled=True)]
where the time goes in v1:
time: 392 us
  waiting for transfers between devices  296 us (76%)
  matrix products  21 us (5%)
  other arithmetic  19.5 us (5%)
  blocking collectives  18.1 us (5%)
  starting transfers between devices  18 us (5%)
  between operations  13.8 us (4%)
  local copies, waits for them, and re-layouts  5.01 us (1%)
    reduce_scatter x3, waiting for transfers between devices, shards(): lax.psum_scatter(partial_out.astype(jnp.bfloat16), 'tp', scatter_dimensio...  93.7 us
    all_to_all x1, waiting for transfers between devices, track_ladders_on_mesh(): lax.all_to_all(jnp.stack([message for _ in range(lax.axis_size('sp'))], a...  79.5 us
    all_gather x3, waiting for transfers between devices, shards(): full_rows = lax.all_gather(stream, 'tp', axis=1, tiled=True)  60 us
    all_gather x1, waiting for transfers between devices, shards(): lax.all_gather(w_out, 'sp', axis=2, tiled=True)  46.6 us
    psum x3, blocking collectives, shards(): lax.psum((jnp.sum(filtered, axis=1), jnp.sum(filtered * filtered, axis=1)...  18.1 us
    dot_general x3, matrix products, shards(): jnp.dot(normed, whole_out[layer], preferred_element_type=jnp.float32)  10.3 us
    all_gather x1, waiting for transfers between devices, shards(): lax.all_gather(w_gate, 'sp', axis=1, tiled=True)  10.2 us
    ppermute x3, starting transfers between devices, from_behind(): return lax.ppermute(block, axis, route)  10.1 us
  transfers between devices with their start and end apart: 12, of which 12 were waited for; matrix products, arithmetic and copies ran while one was open for 3% of the time, Pallas kernels for 0%

profile of v1, /device:TPU:0, one launch (start us, length us, event | category | flops | bytes accessed | tf_op | source)
XLA Modules:
  0.0 391.7 jit_solution(11721775641366779315)
XLA Ops:
  8.0 3.0 stack.2
  11.1 7.4 %all-to-all-start = ((bf16[8,3,256,256]{3,2,1,0:T(8,128)(2,1)}), bf16[8,3,256,256]{3,2,1,0:T(8,128)(2,1)S(1)}, u32[]{:S(2)}, u32[]{:S(2)}) async-start(bf16[8,3,256,256]{3,2,1,0:T(8,128)(2,1)} %stack.2), calls=%async_computation | async-start | bytes 6291456 | tf_op jit(solution)/shard_map/all_to_all | solution.py:10
  19.4 14.8 %all-gather.6.cloned.1.call-done = bf16[512,2048]{1,0:T(8,128)(2,1)} async-done(((bf16[512,512]{1,0:T(8,128)(2,1)}), bf16[512,2048]{1,0:T(8,128)(2,1)}) %all-gather.6.cloned.1.call-update) | async-done | bytes 2097168 | tf_op jit(solution)/shard_map/all_gather | solution.py:38
  36.3 79.5 %all-to-all-done = bf16[8,3,256,256]{3,2,1,0:T(8,128)(2,1)S(1)} async-done(((bf16[8,3,256,256]{3,2,1,0:T(8,128)(2,1)}), bf16[8,3,256,256]{3,2,1,0:T(8,128)(2,1)S(1)}, u32[]{:S(2)}, u32[]{:S(2)}) %all-to-all-start) | async-done | bytes 3145760 | tf_op jit(solution)/shard_map/all_to_all | solution.py:10
  117.5 10.2 %all-gather.8.cloned.1.call-done = bf16[3,2048,256]{2,1,0:T(8,128)(2,1)} async-done(((bf16[3,256,256]{2,1,0:T(8,128)(2,1)}), bf16[3,2048,256]{2,1,0:T(8,128)(2,1)}) %all-gather.8.cloned.1.call-update) | async-done | bytes 3145744 | tf_op jit(solution)/shard_map/all_gather | solution.py:33
  127.7 2.8 fusion.17
  131.3 3.4 collective-permute-start
  136.1 2.4 fusion.134
  138.6 6.3 %all-reduce.2 = (f32[512]{0:T(512)S(1)}, f32[512]{0:T(512)S(1)}) all-reduce(f32[512]{0:T(512)S(1)} %get-tuple-element.10, f32[512]{0:T(512)S(1)} %get-tuple-element.9), channel_id=1, replica_groups=mesh['sp'=8,'tp'=4] {'tp'}, use_global_device_ids=true, to_apply=%region_4.0 | all-reduce | flops 1024 | bytes 8192 | tf_op jit(solution)/shard_map/psum | solution.py:53
  144.8 46.6 %all-gather.10.cloned.1.call-done = bf16[3,256,2048]{2,1,0:T(8,128)(2,1)} async-done(((bf16[3,256,256]{2,1,0:T(8,128)(2,1)}), bf16[3,256,2048]{2,1,0:T(8,128)(2,1)}) %all-gather.10.cloned.1.call-update) | async-done | bytes 3145744 | tf_op jit(solution)/shard_map/all_gather | solution.py:34
  191.4 3.4 convolution_convert_fusion.2
  194.9 29.5 %reduce-scatter.4.cloned.1.call-done = bf16[512,512]{1,0:T(8,128)(2,1)} async-done(((bf16[512,2048]{1,0:T(8,128)(2,1)}), bf16[512,512]{1,0:T(8,128)(2,1)}) %reduce-scatter.4.cloned.1.call-update) | async-done | bytes 524304 | tf_op jit(solution)/shard_map/reduce_scatter | solution.py:63
  226.5 22.6 %all-gather.12.cloned.1.call-done = bf16[512,2048]{1,0:T(8,128)(2,1)} async-done(((bf16[512,512]{1,0:T(8,128)(2,1)}), bf16[512,2048]{1,0:T(8,128)(2,1)}) %all-gather.12.cloned.1.call-update) | async-done | bytes 2097168 | tf_op jit(solution)/shard_map/all_gather | solution.py:38
  251.2 2.8 fusion.14
  254.8 3.4 collective-permute-start.1
  262.1 5.9 %all-reduce.1 = (f32[512]{0:T(512)S(1)}, f32[512]{0:T(512)S(1)}) all-reduce(f32[512]{0:T(512)S(1)} %get-tuple-element.8, f32[512]{0:T(512)S(1)} %get-tuple-element.7), channel_id=1, replica_groups=mesh['sp'=8,'tp'=4] {'tp'}, use_global_device_ids=true, to_apply=%region_10.11 | all-reduce | flops 1024 | bytes 8192 | tf_op jit(solution)/shard_map/psum | solution.py:53
  268.0 3.4 convolution_convert_fusion.1
  271.5 32.1 %reduce-scatter.6.cloned.1.call-done = bf16[512,512]{1,0:T(8,128)(2,1)} async-done(((bf16[512,2048]{1,0:T(8,128)(2,1)}), bf16[512,512]{1,0:T(8,128)(2,1)}) %reduce-scatter.6.cloned.1.call-update) | async-done | bytes 524304 | tf_op jit(solution)/shard_map/reduce_scatter | solution.py:63
  305.8 22.5 %all-gather.14.cloned.1.call-done = bf16[512,2048]{1,0:T(8,128)(2,1)} async-done(((bf16[512,512]{1,0:T(8,128)(2,1)}), bf16[512,2048]{1,0:T(8,128)(2,1)}) %all-gather.14.cloned.1.call-update) | async-done | bytes 2097168 | tf_op jit(solution)/shard_map/all_gather | solution.py:38
  330.4 2.8 fusion.11
  334.0 3.4 collective-permute-start.2
  341.3 5.9 %all-reduce = (f32[512]{0:T(512)S(1)}, f32[512]{0:T(512)S(1)}) all-reduce(f32[512]{0:T(512)S(1)} %get-tuple-element.6, f32[512]{0:T(512)S(1)} %get-tuple-element.5), channel_id=1, replica_groups=mesh['sp'=8,'tp'=4] {'tp'}, use_global_device_ids=true, to_apply=%region_16.17 | all-reduce | flops 1024 | bytes 8192 | tf_op jit(solution)/shard_map/psum | solution.py:53
  347.2 3.5 convolution_convert_fusion
  350.7 32.1 %reduce-scatter.8.cloned.1.call-done = bf16[512,512]{1,0:T(8,128)(2,1)} async-done(((bf16[512,2048]{1,0:T(8,128)(2,1)}), bf16[512,512]{1,0:T(8,128)(2,1)}) %reduce-scatter.8.cloned.1.call-update) | async-done | bytes 524304 | tf_op jit(solution)/shard_map/reduce_scatter | solution.py:63
  (74 shorter events, 28.1 us)
Async XLA Ops:
  6.5 27.7 %all-gather.6.cloned.1.call-start = ((), (), s32[]{:S(2)}) async-start(), calls=%async_computation.4 | async-start | bytes 2621440 | tf_op jit(solution)/shard_map/all_gather | solution.py:38
  7.3 120.4 %all-gather.8.cloned.1.call-start = ((), (), s32[]{:S(2)}) async-start(), calls=%async_computation.5 | async-start | bytes 3538944 | tf_op jit(solution)/shard_map/all_gather | solution.py:33
  11.1 8.2 %copy-start.11 = (f32[3,256]{1,0:T(4,128)S(1)}, f32[3,256]{1,0:T(4,128)}, u32[]{:S(2)}) copy-start(f32[3,256]{1,0:T(4,128)} %param.13) | copy-start | bytes 9220
  11.1 8.2 %copy-start.9 = (f32[3,31,256]{2,1,0:T(8,128)S(1)}, f32[3,31,256]{2,1,0:T(8,128)}, u32[]{:S(2)}) copy-start(f32[3,31,256]{2,1,0:T(8,128)} %param.12) | copy-start | bytes 285700
  11.1 8.3 %copy-start.10 = (f32[3,2048]{1,0:T(4,128)S(1)}, f32[3,2048]{1,0:T(4,128)}, u32[]{:S(2)}) copy-start(f32[3,2048]{1,0:T(4,128)} %param.9) | copy-start | bytes 73732
  11.1 104.7 %all-to-all-start = ((bf16[8,3,256,256]{3,2,1,0:T(8,128)(2,1)}), bf16[8,3,256,256]{3,2,1,0:T(8,128)(2,1)S(1)}, u32[]{:S(2)}, u32[]{:S(2)}) async-start(bf16[8,3,256,256]{3,2,1,0:T(8,128)(2,1)} %stack.2), calls=%async_computation | async-start | bytes 6291456 | tf_op jit(solution)/shard_map/all_to_all | solution.py:10
  18.5 173.0 %all-gather.10.cloned.1.call-start = ((), (), s32[]{:S(2)}) async-start(), calls=%async_computation.6 | async-start | bytes 3538944 | tf_op jit(solution)/shard_map/all_gather | solution.py:34
  19.2 205.2 %reduce-scatter.4.cloned.1.call-start = ((), (), s32[]{:S(2)}) async-start(), calls=%async_computation.7 | async-start | bytes 2621440 | tf_op jit(solution)/shard_map/reduce_scatter | solution.py:63
  127.7 2.8 copy-start.8
  130.5 4.2 %copy-start.12 = (f32[3,256]{1,0:T(4,128)S(1)}, f32[3,256]{1,0:T(4,128)}, u32[]{:S(2)}) copy-start(f32[3,256]{1,0:T(4,128)} %param.14) | copy-start | bytes 9220
  131.3 4.8 %collective-permute-start = (bf16[30,256]{1,0:T(8,128)(2,1)S(1)}, bf16[30,256]{1,0:T(8,128)(2,1)S(1)}, u32[]{:S(2)}, u32[]{:S(2)}) collective-permute-start(bf16[30,256]{1,0:T(8,128)(2,1)S(1)} %slice.821), channel_id=1, source_target_pairs={{0,4},{4,8},{8,12},{12,16},{16,20},{20,24},{24,28},{1,5},{5,9},{9,... | collective-permute-start | bytes 46088 | tf_op jit(solution)/shard_map/ppermute | solution.py:23
  191.4 33.0 %copy-start.2 = (bf16[512,512]{1,0:T(8,128)(2,1)S(1)}, bf16[512,512]{1,0:T(8,128)(2,1)}, u32[]{:S(2)}) copy-start(bf16[512,512]{1,0:T(8,128)(2,1)} %param.8) | copy-start | bytes 1572868
  194.9 54.2 %all-gather.12.cloned.1.call-start = ((), (), s32[]{:S(2)}) async-start(), calls=%async_computation.8 | async-start | bytes 2621440 | tf_op jit(solution)/shard_map/all_gather | solution.py:38
  226.4 77.2 %reduce-scatter.6.cloned.1.call-start = ((), (), s32[]{:S(2)}) async-start(), calls=%async_computation.9 | async-start | bytes 2621440 | tf_op jit(solution)/shard_map/reduce_scatter | solution.py:63
  251.2 2.8 copy-start.4
  251.2 2.8 copy-start.7
  254.8 4.8 %collective-permute-start.1 = (bf16[30,256]{1,0:T(8,128)(2,1)S(1)}, bf16[30,256]{1,0:T(8,128)(2,1)S(1)}, u32[]{:S(2)}, u32[]{:S(2)}) collective-permute-start(bf16[30,256]{1,0:T(8,128)(2,1)S(1)} %slice.883), channel_id=1, source_target_pairs={{0,4},{4,8},{8,12},{12,16},{16,20},{20,24},{24,28},{1,5},{5,9},{9,... | collective-permute-start | bytes 46088 | tf_op jit(solution)/shard_map/ppermute | solution.py:23
  268.0 35.6 %copy-start = (bf16[512,512]{1,0:T(8,128)(2,1)S(1)}, bf16[512,512]{1,0:T(8,128)(2,1)}, u32[]{:S(2)}) copy-start(bf16[512,512]{1,0:T(8,128)(2,1)} %add_convert_fusion.2) | copy-start | bytes 1572868
  271.5 56.9 %all-gather.14.cloned.1.call-start = ((), (), s32[]{:S(2)}) async-start(), calls=%async_computation.10 | async-start | bytes 2621440 | tf_op jit(solution)/shard_map/all_gather | solution.py:38
  305.6 77.2 %reduce-scatter.8.cloned.1.call-start = ((), (), s32[]{:S(2)}) async-start(), calls=%async_computation.11 | async-start | bytes 2621440 | tf_op jit(solution)/shard_map/reduce_scatter | solution.py:63
  330.4 2.8 copy-start.5
  330.4 2.8 copy-start.6
  334.0 4.8 %collective-permute-start.2 = (bf16[30,256]{1,0:T(8,128)(2,1)S(1)}, bf16[30,256]{1,0:T(8,128)(2,1)S(1)}, u32[]{:S(2)}, u32[]{:S(2)}) collective-permute-start(bf16[30,256]{1,0:T(8,128)(2,1)S(1)} %slice.945), channel_id=1, source_target_pairs={{0,4},{4,8},{8,12},{12,16},{16,20},{20,24},{24,28},{1,5},{5,9},{9,... | collective-permute-start | bytes 46088 | tf_op jit(solution)/shard_map/ppermute | solution.py:23
  347.2 35.6 %copy-start.1 = (bf16[512,512]{1,0:T(8,128)(2,1)S(1)}, bf16[512,512]{1,0:T(8,128)(2,1)}, u32[]{:S(2)}) copy-start(bf16[512,512]{1,0:T(8,128)(2,1)} %add_convert_fusion.1) | copy-start | bytes 1572868
  (1 other events, 2.8 us)
Sparse Core Ops, SparseCore 0:
  8.9 25.2 all-gather.5
  36.4 91.2 all-gather.7
  129.7 61.6 all-gather.9
  195.0 29.3 reduce-scatter.3
  226.5 22.5 all-gather.11
  271.6 31.9 reduce-scatter.5
  305.7 22.5 all-gather.13
  350.8 31.9 reduce-scatter.7
